TPU v7x, 512 devices: a whole 4x8x8 slice. The times are simulated.
512 devices in a mesh: sp: 32 (over z, x), tp: 16 (over y, core).
Axes of the slice: x: 4, y: 8, z: 8, core: 2. Of those that a mesh axis runs over, the one named last changes fastest.
Arguments:
- moe_in: bfloat16 [6144, 2048], P('sp', 'tp'), may hold values from -6 to 6
- cotangent: bfloat16 [6144, 2048], P('sp', 'tp'), may hold values from -6 to 6
- routes: int32 [6144, 2], P('sp'), may hold values from 0 to 31, all different within a row; in each aligned block of 192 rows (0 to 191, 192 to 383, ...) at most 15 rows name the same one
- route_weight: float32 [6144, 2], P('sp'), may hold values from 0.2 to 1
- w_gate: bfloat16 [32, 3584, 2048], P('sp', 'tp'), may hold values from -0.125 to 0.125
- w_up: bfloat16 [32, 3584, 2048], P('sp', 'tp'), may hold values from -0.125 to 0.125
- w_down: bfloat16 [32, 3584, 2048], P('sp', 'tp'), may hold values from -0.09375 to 0.09375
- conv_pre: bfloat16 [6144, 2048], P('sp', 'tp'), may hold values from -6 to 6
- norm_mean: float32 [6144], P('sp'), may hold values from -3 to 3
- norm_rstd: float32 [6144], P('sp'), may hold values from 0.5 to 2
- ln_gain: float32 [2048], P('tp'), may hold values from 0.1 to 1.9
- ln_shift: float32 [2048], P('tp'), may hold values from -3 to 3
- taps: float32 [31, 2048], P(None, 'tp'), may hold values from -1 to 1
- w_proj: bfloat16 [2048, 2048], P('sp', 'tp'), may hold values from -0.125 to 0.125
Outputs:
- grad_up: bfloat16 [32, 3584, 2048], P('sp', 'tp')
- grad_down: bfloat16 [32, 3584, 2048], P('sp', 'tp')
- grad_stream: bfloat16 [6144, 2048], P('sp', 'tp')
- grad_proj: float32 [2048, 2048], P('sp', 'tp')
- grad_conv: bfloat16 [6144, 2048], P('sp', 'tp')
Inputs may be any that keep to these rules, and one draw needn't show every extreme that they name: `routes`: each token names 2 different experts. Among the tokens of one index of sp no expert is named more than 15 times, a bound that some block reaches.
All inputs are finite; a program needn't handle non-finite values.
Results may differ from a plain program's by a relative error of at most 0.02.
Values may be sent and summed in bfloat16 or wider, within the bound.
A program may use at most 64 MiB of HBM per device.

v0:
```python
import jax
import jax.numpy as jnp
from jax import lax
from jax.sharding import PartitionSpec as P


def sent_together(arrays, axis, split_dim, concat_dim, along):
    ends, at = ([], 0)
    for a in arrays[:-1]:
        at += a.shape[along]
        ends.append(at)
    both = jnp.concatenate(arrays, axis=along)
    return tuple(
        jnp.split(
            lax.all_to_all(both, axis, split_axis=split_dim, concat_axis=concat_dim, tiled=True),
            ends,
            axis=along,
        )
    )


def side_by_side(arrays, axis, dim, along):
    widths = [a.shape[along] for a in arrays]
    both = jnp.concatenate(arrays, axis=along)
    out = lax.all_gather(both, axis, axis=dim, tiled=True)
    return tuple(jnp.split(out, [sum(widths[:k]) for k in range(1, len(widths))], axis=along))


def in_blocks(value, dim, devices):
    before, after = (value.shape[:dim], value.shape[dim + 1 :])
    return jnp.moveaxis(value.reshape(*before, devices, -1, *after), dim, 0)


def summed_on_arrival(value, axis, dim):
    blocks = in_blocks(value, dim, lax.axis_size(axis))
    arrived = lax.all_to_all(blocks, axis, split_axis=0, concat_axis=0, tiled=True)
    return arrived.astype(jnp.float32).sum(axis=0)


def joined_along(blocks, dim):
    dims = list(blocks.shape[1:])
    dims[dim] *= blocks.shape[0]
    return jnp.moveaxis(blocks, 0, dim).reshape(dims)


def sent_to_all(value, axis):
    copies = jnp.broadcast_to(value, (lax.axis_size(axis), *value.shape))
    return lax.all_to_all(copies, axis, split_axis=0, concat_axis=0, tiled=True)


def gather_directly(value, axis, dim):
    return joined_along(sent_to_all(value, axis), dim)


def taken_together(value, axis):
    everything = sent_to_all(value, axis)
    return jnp.sum(everything, axis=0)


def in_one(arrays, axis):
    ravelled, at, finished = (jnp.concatenate([a.reshape(-1) for a in arrays]), 0, [])
    subtotal = taken_together(ravelled, axis)
    for a in arrays:
        finished.append(subtotal[at : at + a.size].reshape(a.shape))
        at += a.size
    return tuple(finished)


def passed_along(value, axis, steps):
    count = lax.axis_size(axis)
    first, last = (max(0, -steps), min(count, count - steps))
    return lax.ppermute(value, axis, [(source, source + steps) for source in range(first, last)])


def silu_slope(pre_value, sigmoid_value):
    return sigmoid_value * (1.0 + pre_value * (1.0 - sigmoid_value))


def expert_backward(expert_rows, routed_rows, gate_weight, up_weight, down_weight):
    gate_pre = lax.dot_general(
        expert_rows, gate_weight, (((1,), (1,)), ((), ())), preferred_element_type=jnp.float32
    )
    up_pre = lax.dot_general(
        expert_rows, up_weight, (((1,), (1,)), ((), ())), preferred_element_type=jnp.float32
    )
    gate_sigmoid = jax.nn.sigmoid(gate_pre)
    gate_active = gate_pre * gate_sigmoid
    hidden = (gate_active * up_pre).astype(jnp.bfloat16)
    hidden_grad = lax.dot_general(
        routed_rows, down_weight, (((1,), (1,)), ((), ())), preferred_element_type=jnp.float32
    )
    grad_down = lax.dot_general(
        hidden, routed_rows, (((0,), (0,)), ((), ())), preferred_element_type=jnp.float32
    ).astype(jnp.bfloat16)
    gate_grad = (hidden_grad * up_pre * silu_slope(gate_pre, gate_sigmoid)).astype(jnp.bfloat16)
    up_grad = (hidden_grad * gate_active).astype(jnp.bfloat16)
    grad_up = lax.dot_general(
        up_grad, expert_rows, (((0,), (0,)), ((), ())), preferred_element_type=jnp.float32
    ).astype(jnp.bfloat16)
    partial_rows = jnp.dot(gate_grad, gate_weight, preferred_element_type=jnp.float32)
    partial_rows = partial_rows + jnp.dot(up_grad, up_weight, preferred_element_type=jnp.float32)
    return (grad_up[None], grad_down[None], partial_rows)


def on_device(
    moe_in,
    cotangent,
    routes,
    route_weight,
    w_gate,
    w_up,
    w_down,
    conv_pre,
    norm_mean,
    norm_rstd,
    ln_gain,
    ln_shift,
    taps,
    w_proj,
):
    devices = lax.axis_size("sp")
    local_tokens = routes.shape[0]
    top_count = routes.shape[1]
    channels = moe_in.shape[1]
    capacity = 5 * local_tokens // (2 * devices)
    route_ids = routes.reshape(-1)
    onehot = (route_ids[:, None] == jnp.arange(devices, dtype=jnp.int32)[None, :]).astype(jnp.int32)
    earlier = jnp.cumsum(onehot, axis=0) - onehot
    targets = route_ids * capacity + jnp.sum(earlier * onehot, axis=1)
    positions = jnp.arange(devices * capacity, dtype=jnp.int32)
    matches = targets[None, :] == positions[:, None]
    filled = jnp.any(matches, axis=1)[:, None]
    pair_index = jnp.arange(targets.shape[0], dtype=jnp.int32)
    route_of_slot = jnp.sum(jnp.where(matches, pair_index[None, :], 0), axis=1)
    zero_value = jnp.zeros((), jnp.bfloat16)
    routed = (route_weight[:, :, None] * cotangent.astype(jnp.float32)[:, None, :]).astype(
        jnp.bfloat16
    )
    routed = routed.reshape(local_tokens * top_count, cotangent.shape[1])
    send_rows = jnp.where(filled, jnp.take(moe_in, route_of_slot // top_count, axis=0), zero_value)
    send_routed = jnp.where(filled, jnp.take(routed, route_of_slot, axis=0), zero_value)
    send_rows, send_routed = (send_rows, send_routed)
    part_rows, part_routed = sent_together((send_rows, send_routed), "sp", 0, 0, 1)
    expert_rows, routed_rows = side_by_side((part_rows, part_routed), "tp", 1, 0)
    grad_up, grad_down, partial_rows = expert_backward(
        expert_rows, routed_rows, w_gate[0], w_up[0], w_down[0]
    )
    shared = summed_on_arrival(
        partial_rows.astype(jnp.bfloat16).astype(jnp.float32).astype(jnp.bfloat16), "tp", 1
    ).astype(jnp.bfloat16)
    returned = lax.all_to_all(shared, "sp", split_axis=0, concat_axis=0, tiled=True)
    picked = jnp.take(returned, targets, axis=0).astype(jnp.float32)
    grad_stream = (
        cotangent.astype(jnp.float32)
        + jnp.sum(picked.reshape(local_tokens, top_count, returned.shape[1]), axis=1)
    ).astype(jnp.bfloat16)
    mix_grad = lax.all_gather(grad_stream, "tp", axis=1, tiled=True)
    normed = (conv_pre.astype(jnp.float32) - norm_mean[:, None]) * norm_rstd[:, None]
    pre_act = normed * ln_gain[None, :] + ln_shift[None, :]
    act_sigmoid = jax.nn.sigmoid(pre_act)
    activated = (pre_act * act_sigmoid).astype(jnp.bfloat16)
    columns = mix_grad
    act_grad = jnp.dot(
        columns, gather_directly(w_proj, "sp", 0), preferred_element_type=jnp.float32
    )
    columns = mix_grad
    grad_proj = summed_on_arrival(
        lax.dot_general(
            columns, activated, (((0,), (0,)), ((), ())), preferred_element_type=jnp.float32
        ).astype(jnp.bfloat16),
        "sp",
        0,
    )
    normed_grad = act_grad * silu_slope(pre_act, act_sigmoid) * ln_gain[None, :]
    first_sum, second_sum = in_one(
        (jnp.sum(normed_grad, axis=1), jnp.sum(normed_grad * normed, axis=1)), "tp"
    )
    width = channels * lax.axis_size("tp")
    conv_grad = norm_rstd[:, None] * (
        normed_grad - first_sum[:, None] / width - normed * (second_sum[:, None] / width)
    )
    lag_count = taps.shape[0]
    rim_rows = passed_along(conv_grad[: lag_count - 1], "sp", -1)
    extended = jnp.concatenate([conv_grad, rim_rows], axis=0)
    grad_conv = jnp.zeros((local_tokens, channels), jnp.float32)
    for lag in range(lag_count):
        grad_conv = grad_conv + taps[lag][None, :] * extended[lag : lag + local_tokens]
    return (grad_up, grad_down, grad_stream, grad_proj, grad_conv.astype(jnp.bfloat16))


def solution(mesh):
    placed = (
        P("sp", "tp"),
        P("sp", "tp"),
        P("sp", None),
        P("sp", None),
        P("sp", "tp", None),
        P("sp", "tp", None),
        P("sp", "tp", None),
        P("sp", "tp"),
        P("sp"),
        P("sp"),
        P("tp"),
        P("tp"),
        P(None, "tp"),
        P("sp", "tp"),
    )
    return jax.shard_map(
        on_device,
        mesh=mesh,
        in_specs=placed,
        out_specs=(
            P("sp", "tp", None),
            P("sp", "tp", None),
            P("sp", "tp"),
            P("sp", "tp"),
            P("sp", "tp"),
        ),
        check_vma=False,
    )
```

profile of v0, /device:TPU:1, one launch (start us, length us, event | category | flops | bytes accessed | tf_op | source)
XLA Modules:
  0.0 246.9 jit_solution(16162879522349706019)
XLA Ops:
  10.1 2.0 gather_fusion
  14.3 1.5 gather_fusion.1
  16.2 24.8 %all_to_all.42 = bf16[32,15,256]{2,1,0:T(8,128)(2,1)S(1)} all-to-all(bf16[32,15,256]{2,1,0:T(8,128)(2,1)S(1)} %pad_maximum_fusion), channel_id=1, replica_groups=mesh['sp'=32,'tp'=16] {'sp'}, dimensions={0} | all-to-all | bytes 491520 | tf_op jit(solution)/shard_map/all_to_all | solution.py:15
  41.9 49.1 %all-gather.2.cloned.1.call-done = bf16[960,2048]{1,0:T(8,128)(2,1)} async-done(((bf16[960,128]{1,0:T(8,128)(2,1)}), bf16[960,2048]{1,0:T(8,128)(2,1)}) %all-gather.2.cloned.1.call-update) | async-done | bytes 3932176 | tf_op jit(solution)/shard_map/all_gather | solution.py:25
  91.0 2.4 fusion.9
  97.3 1.6 copy.60
  98.9 3.8 %all-to-all-start.1 = ((bf16[16,480,128]{2,1,0:T(8,128)(2,1)}), bf16[16,480,128]{2,1,0:T(8,128)(2,1)S(1)}, u32[]{:S(2)}, u32[]{:S(2)}) async-start(bf16[16,480,128]{2,1,0:T(8,128)(2,1)} %bitcast.121), calls=%async_computation.1 | async-start | bytes 3932160 | tf_op jit(solution)/shard_map/all_to_all | solution.py:36
  103.2 45.9 %all-to-all-done.1 = bf16[16,480,128]{2,1,0:T(8,128)(2,1)S(1)} async-done(((bf16[16,480,128]{2,1,0:T(8,128)(2,1)}), bf16[16,480,128]{2,1,0:T(8,128)(2,1)S(1)}, u32[]{:S(2)}, u32[]{:S(2)}) %all-to-all-start.1) | async-done | bytes 1966112 | tf_op jit(solution)/shard_map/all_to_all | solution.py:36
  150.2 9.7 %all-to-all-start.2 = ((bf16[32,15,128]{2,1,0:T(8,128)(2,1)}), bf16[32,15,128]{2,1,0:T(8,128)(2,1)S(1)}, u32[]{:S(2)}, u32[]{:S(2)}) async-start(bf16[32,15,128]{2,1,0:T(8,128)(2,1)} %all_to_all.30), calls=%async_computation.2 | async-start | bytes 262144 | tf_op jit(solution)/shard_map/all_to_all | solution.py:151
  159.9 1.6 slice_bitcast_fusion.29
  161.5 8.3 %all-to-all-done.2 = bf16[32,15,128]{2,1,0:T(8,128)(2,1)S(1)} async-done(((bf16[32,15,128]{2,1,0:T(8,128)(2,1)}), bf16[32,15,128]{2,1,0:T(8,128)(2,1)S(1)}, u32[]{:S(2)}, u32[]{:S(2)}) %all-to-all-start.2) | async-done | bytes 122912 | tf_op jit(solution)/shard_map/all_to_all | solution.py:151
  169.8 1.6 broadcast_in_dim.97
  171.4 4.8 %all-to-all-start.4 = ((bf16[32,64,128]{2,1,0:T(8,128)(2,1)}), bf16[32,64,128]{2,1,0:T(8,128)(2,1)}, u32[]{:S(2)}, u32[]{:S(2)}) async-start(bf16[32,64,128]{2,1,0:T(8,128)(2,1)} %broadcast_in_dim.97), calls=%async_computation.4 | async-start | bytes 1048576 | tf_op jit(solution)/shard_map/all_to_all | solution.py:48
  177.1 1.4 gather_fusion.2
  179.0 18.7 %all_gather.7 = bf16[192,2048]{1,0:T(8,128)(2,1)S(1)} all-gather(bf16[192,128]{1,0:T(8,128)(2,1)S(1)} %add_convert_fusion.1), channel_id=1, replica_groups=mesh['sp'=32,'tp'=16] {'tp'}, dimensions={1}, use_global_device_ids=true | all-gather | bytes 835584 | tf_op jit(solution)/shard_map/all_gather | solution.py:157
  197.6 1.6 fusion.127
  199.9 6.0 %all-to-all-start.5 = ((f32[16,1,384]{2,1,0:T(1,128)}), f32[16,1,384]{2,1,0:T(1,128)S(1)}, u32[]{:S(2)}, u32[]{:S(2)}) async-start(f32[16,1,384]{2,1,0:T(1,128)} %broadcast_in_dim.98), calls=%async_computation.5 | async-start | bytes 49152 | tf_op jit(solution)/shard_map/all_to_all | solution.py:48
  205.9 2.1 convolution_convert_fusion.2
  208.0 5.2 %all-to-all-done.5 = f32[16,1,384]{2,1,0:T(1,128)S(1)} async-done(((f32[16,1,384]{2,1,0:T(1,128)}), f32[16,1,384]{2,1,0:T(1,128)S(1)}, u32[]{:S(2)}, u32[]{:S(2)}) %all-to-all-start.5) | async-done | bytes 24608 | tf_op jit(solution)/shard_map/all_to_all | solution.py:48
  213.3 9.4 %all-to-all-start.3 = ((bf16[32,64,128]{2,1,0:T(8,128)(2,1)}), bf16[32,64,128]{2,1,0:T(8,128)(2,1)S(1)}, u32[]{:S(2)}, u32[]{:S(2)}) async-start(bf16[32,64,128]{2,1,0:T(8,128)(2,1)} %bitcast.123), calls=%async_computation.3 | async-start | bytes 1048576 | tf_op jit(solution)/shard_map/all_to_all | solution.py:36
  223.0 3.1 %fusion.1 = bf16[1,224,2048]{2,1,0:T(8,128)(2,1)} fusion(bf16[960,2048]{1,0:T(8,128)(2,1)} %all-gather.2.cloned.1.call-done, f32[480,224]{0,1:T(8,128)S(1)} %copy-done.2, f32[480,224]{0,1:T(8,128)S(1)} %fusion.9), kind=kOutput, calls=%fused_computation.7 | convolution fusion | flops 441505792 | bytes 3743744 | tf_op jit(solution)/shard_map/dot_general | solution.py:92
  226.5 1.3 collective-permute-start
  227.8 3.1 %fusion = bf16[1,224,2048]{2,1,0:T(8,128)(2,1)} fusion(bf16[480,224]{0,1:T(8,128)(2,1)S(1)} %copy-done.5, bf16[960,2048]{1,0:T(8,128)(2,1)} %all-gather.2.cloned.1.call-done), kind=kOutput, calls=%fused_computation.6 | convolution fusion | flops 440860672 | bytes 3098624 | tf_op jit(solution)/shard_map/dot_general | solution.py:97
  232.9 6.4 %all-to-all-done.3 = bf16[32,64,128]{2,1,0:T(8,128)(2,1)S(1)} async-done(((bf16[32,64,128]{2,1,0:T(8,128)(2,1)}), bf16[32,64,128]{2,1,0:T(8,128)(2,1)S(1)}, u32[]{:S(2)}, u32[]{:S(2)}) %all-to-all-start.3) | async-done | bytes 524320 | tf_op jit(solution)/shard_map/all_to_all | solution.py:36
  (149 shorter events, 16.4 us)
Async XLA Ops:
  7.2 83.8 %copy-start = (bf16[1,224,2048]{2,1,0:T(8,128)(2,1)S(1)}, bf16[1,224,2048]{2,1,0:T(8,128)(2,1)}, u32[]{:S(2)}) copy-start(bf16[1,224,2048]{2,1,0:T(8,128)(2,1)} %param.18) | copy-start | bytes 2752516
  7.2 83.8 %all-gather.2.cloned.1.call-start = ((), (), s32[]{:S(2)}) async-start(), calls=%async_computation.6 | async-start | bytes 4177920 | tf_op jit(solution)/shard_map/all_gather | solution.py:25
  41.1 52.3 %copy-start.3 = (bf16[1,224,2048]{2,1,0:T(8,128)(2,1)S(1)}, bf16[1,224,2048]{2,1,0:T(8,128)(2,1)}, u32[]{:S(2)}) copy-start(bf16[1,224,2048]{2,1,0:T(8,128)(2,1)} %param.19) | copy-start | bytes 2752516
  98.9 50.2 %all-to-all-start.1 = ((bf16[16,480,128]{2,1,0:T(8,128)(2,1)}), bf16[16,480,128]{2,1,0:T(8,128)(2,1)S(1)}, u32[]{:S(2)}, u32[]{:S(2)}) async-start(bf16[16,480,128]{2,1,0:T(8,128)(2,1)} %bitcast.121), calls=%async_computation.1 | async-start | bytes 3932160 | tf_op jit(solution)/shard_map/all_to_all | solution.py:36
  103.1 73.2 %copy-start.11 = (f32[31,128]{1,0:T(8,128)S(1)}, f32[31,128]{1,0:T(8,128)}, u32[]{:S(2)}) copy-start(f32[31,128]{1,0:T(8,128)} %param.26) | copy-start | bytes 47620
  103.1 75.8 %copy-start.7 = (bf16[192,128]{1,0:T(8,128)(2,1)S(1)}, bf16[192,128]{1,0:T(8,128)(2,1)}, u32[]{:S(2)}) copy-start(bf16[192,128]{1,0:T(8,128)(2,1)} %param.15) | copy-start | bytes 147460
  149.4 48.2 %copy-start.8 = (bf16[192,128]{1,0:T(8,128)(2,1)S(1)}, bf16[192,128]{1,0:T(8,128)(2,1)}, u32[]{:S(2)}) copy-start(bf16[192,128]{1,0:T(8,128)(2,1)} %param.21) | copy-start | bytes 147460
  150.2 19.6 %all-to-all-start.2 = ((bf16[32,15,128]{2,1,0:T(8,128)(2,1)}), bf16[32,15,128]{2,1,0:T(8,128)(2,1)S(1)}, u32[]{:S(2)}, u32[]{:S(2)}) async-start(bf16[32,15,128]{2,1,0:T(8,128)(2,1)} %all_to_all.30), calls=%async_computation.2 | async-start | bytes 262144 | tf_op jit(solution)/shard_map/all_to_all | solution.py:151
  171.4 51.3 %copy-start.2 = (f32[480,224]{0,1:T(8,128)S(1)}, f32[480,224]{0,1:T(8,128)}, u32[]{:S(2)}) copy-start(f32[480,224]{0,1:T(8,128)} %copy-done.1) | copy-start | bytes 1290244
  171.4 26.2 %all-to-all-start.4 = ((bf16[32,64,128]{2,1,0:T(8,128)(2,1)}), bf16[32,64,128]{2,1,0:T(8,128)(2,1)}, u32[]{:S(2)}, u32[]{:S(2)}) async-start(bf16[32,64,128]{2,1,0:T(8,128)(2,1)} %broadcast_in_dim.97), calls=%async_computation.4 | async-start | bytes 1048576 | tf_op jit(solution)/shard_map/all_to_all | solution.py:48
  179.0 47.2 %copy-start.6 = (bf16[192,128]{1,0:T(8,128)(2,1)}, bf16[192,128]{1,0:T(8,128)(2,1)S(1)}, u32[]{:S(2)}) copy-start(bf16[192,128]{1,0:T(8,128)(2,1)S(1)} %add_convert_fusion.1) | copy-start | bytes 147460
  199.9 13.4 %all-to-all-start.5 = ((f32[16,1,384]{2,1,0:T(1,128)}), f32[16,1,384]{2,1,0:T(1,128)S(1)}, u32[]{:S(2)}, u32[]{:S(2)}) async-start(f32[16,1,384]{2,1,0:T(1,128)} %broadcast_in_dim.98), calls=%async_computation.5 | async-start | bytes 49152 | tf_op jit(solution)/shard_map/all_to_all | solution.py:48
  205.9 21.9 %copy-start.5 = (bf16[480,224]{0,1:T(8,128)(2,1)S(1)}, bf16[480,224]{0,1:T(8,128)(2,1)}, u32[]{:S(2)}) copy-start(bf16[480,224]{0,1:T(8,128)(2,1)} %copy-done.4) | copy-start | bytes 645124
  208.0 18.2 %copy-start.9 = (bf16[192,128]{1,0:T(8,128)(2,1)S(1)}, bf16[192,128]{1,0:T(8,128)(2,1)}, u32[]{:S(2)}) copy-start(bf16[192,128]{1,0:T(8,128)(2,1)} %param.21) | copy-start | bytes 147460
  208.0 18.2 %copy-start.41 = (f32[192]{0:T(256)S(1)}, f32[192]{0:T(256)}, u32[]{:S(2)}) copy-start(f32[192]{0:T(256)} %param.23) | copy-start | bytes 2308
  208.0 18.2 %copy-start.42 = (f32[192]{0:T(256)S(1)}, f32[192]{0:T(256)}, u32[]{:S(2)}) copy-start(f32[192]{0:T(256)} %param.22) | copy-start | bytes 2308
  213.3 26.0 %all-to-all-start.3 = ((bf16[32,64,128]{2,1,0:T(8,128)(2,1)}), bf16[32,64,128]{2,1,0:T(8,128)(2,1)S(1)}, u32[]{:S(2)}, u32[]{:S(2)}) async-start(bf16[32,64,128]{2,1,0:T(8,128)(2,1)} %bitcast.123), calls=%async_computation.3 | async-start | bytes 1048576 | tf_op jit(solution)/shard_map/all_to_all | solution.py:36
  222.7 9.0 %copy-start.12 = (f32[128]{0:T(128)S(1)}, f32[128]{0:T(128)}, u32[]{:S(2)}) copy-start(f32[128]{0:T(128)} %get-tuple-element.30) | copy-start | bytes 1540
  222.7 9.0 %copy-start.13 = (f32[128]{0:T(128)S(1)}, f32[128]{0:T(128)}, u32[]{:S(2)}) copy-start(f32[128]{0:T(128)} %get-tuple-element.31) | copy-start | bytes 1540
  222.7 9.0 %copy-start.14 = (f32[128]{0:T(128)S(1)}, f32[128]{0:T(128)}, u32[]{:S(2)}) copy-start(f32[128]{0:T(128)} %get-tuple-element.32) | copy-start | bytes 1540
  222.7 9.0 %copy-start.15 = (f32[128]{0:T(128)S(1)}, f32[128]{0:T(128)}, u32[]{:S(2)}) copy-start(f32[128]{0:T(128)} %get-tuple-element.33) | copy-start | bytes 1540
  222.8 9.0 %copy-start.16 = (f32[128]{0:T(128)S(1)}, f32[128]{0:T(128)}, u32[]{:S(2)}) copy-start(f32[128]{0:T(128)} %get-tuple-element.34) | copy-start | bytes 1540
  222.8 9.0 %copy-start.17 = (f32[128]{0:T(128)S(1)}, f32[128]{0:T(128)}, u32[]{:S(2)}) copy-start(f32[128]{0:T(128)} %get-tuple-element.35) | copy-start | bytes 1540
  226.5 5.3 %collective-permute-start = (f32[30,128]{1,0:T(8,128)S(1)}, f32[30,128]{1,0:T(8,128)S(1)}, u32[]{:S(2)}, u32[]{:S(2)}) collective-permute-start(f32[30,128]{1,0:T(8,128)S(1)} %slice.271), channel_id=1, source_target_pairs={{16,0},{32,16},{48,32},{64,48},{80,64},{96,80},{112,96},{128,112},... | collective-permute-start | bytes 46088 | tf_op jit(solution)/shard_map/ppermute | solution.py:72
  (28 other events, 218.2 us)
Sparse Core Ops, SparseCore 0:
  42.0 48.9 all-gather.1
where the time goes:
time: 248 us; the launch traced here: 247 us
  waiting for transfers between devices  116 us (47%)
  blocking collectives  43.5 us (18%)
  starting transfers between devices  35 us (14%)
  local copies, waits for them, and re-layouts  17 us (7%)
  matrix products  15.5 us (6%)
  between operations  14.9 us (6%)
  other arithmetic  5.23 us (2%)
    all_to_all x2, waiting for transfers between devices, summed_on_arrival(): lax.all_to_all(blocks, axis, split_axis=0, concat_axis=0, tiled=True)  52.3 us
    all_gather x1, waiting for transfers between devices, side_by_side(): out = lax.all_gather(both, axis, axis=dim, tiled=True)  49.1 us
    all_to_all x1, blocking collectives, sent_together(): lax.all_to_all(both, axis, split_axis=split_dim, concat_axis=concat_dim,...  24.8 us
    all_gather x1, blocking collectives, on_device(): mix_grad = lax.all_gather(grad_stream, 'tp', axis=1, tiled=True)  18.7 us
    all_to_all x2, starting transfers between devices, summed_on_arrival(): lax.all_to_all(blocks, axis, split_axis=0, concat_axis=0, tiled=True)  13.2 us
    all_to_all x2, starting transfers between devices, sent_to_all(): return lax.all_to_all(copies, axis, split_axis=0, concat_axis=0, tiled=True)  10.7 us
    all_to_all x1, starting transfers between devices, on_device(): lax.all_to_all(shared, 'sp', split_axis=0, concat_axis=0, tiled=True)  9.73 us
    all_to_all x1, waiting for transfers between devices, on_device(): lax.all_to_all(shared, 'sp', split_axis=0, concat_axis=0, tiled=True)  8.31 us
  transfers between devices with their start and end apart: 7, of which 6 were waited for; matrix products, arithmetic and copies ran while one was open for 6% of the time, Pallas kernels for 0%

commit v1 on v0

v1 whole, which is shorter than its diff:
```python
import functools

import jax
import jax.numpy as jnp
from jax import lax
from jax.experimental import pallas as pl
from jax.experimental.pallas import tpu as pltpu
from jax.sharding import PartitionSpec as P

MESH = pl.DeviceIdType.MESH
F32 = jnp.float32
BF16 = jnp.bfloat16
SLOTS = 16
NX = 4
GP = 4


def rcopy(src, dst, ssem, rsem, dev):
    return pltpu.make_async_remote_copy(
        src_ref=src, dst_ref=dst, send_sem=ssem, recv_sem=rsem, device_id=dev, device_id_type=MESH
    )


def nt(a, b):
    return lax.dot_general(a, b, (((1,), (1,)), ((), ())), preferred_element_type=F32)


def nn(a, b):
    return lax.dot_general(a, b, (((1,), (0,)), ((), ())), preferred_element_type=F32)


def tn(a, b):
    return lax.dot_general(a, b, (((0,), (0,)), ((), ())), preferred_element_type=F32)


def silu_slope(pre_value, sigmoid_value):
    return sigmoid_value * (1.0 + pre_value * (1.0 - sigmoid_value))


def sigmoid(v):
    return 1.0 / (1.0 + jnp.exp(-v))


def kernel(
    nsp,
    ntp,
    moe_ref,
    cot_ref,
    routes_ref,
    rw_ref,
    wg_hbm,
    wu_hbm,
    wd_hbm,
    conv_ref,
    mean_ref,
    rstd_ref,
    gain_ref,
    shift_ref,
    taps_ref,
    wproj_ref,
    gup_hbm,
    gdown_hbm,
    gs_out,
    gproj_out,
    gconv_out,
    pack,
    gath,
    wg,
    wu,
    wd,
    acc_g,
    acc_u,
    acc_h,
    hid,
    gg,
    ug,
    gup,
    gdown,
    mine,
    d2d_out,
    d2d_in,
    cw_in,
    ccw_in,
    cw_out,
    ccw_out,
    fin,
    back,
    wp,
    gsa,
    gp,
    gr,
    sums,
    ng_ref,
    ext,
    rim_in,
    w_sem,
    out_sem,
    a2a_s,
    a2a_r,
    nb_r,
    cw_s,
    ccw_s,
    par_s,
    par_r,
    wp_s,
    wp_r,
    d2_s,
    d2_r,
    rcw_s,
    rccw_s,
    rcw_r,
    rccw_r,
    ret_s,
    ret_r,
    gn_r,
    gcw_s,
    gccw_s,
    gpar_s,
    gpar_r,
    gp_s,
    gp_r,
    ar_s,
    ar_r,
    rim_s,
    rim_r,
):
    nz = nsp // NX
    ny = ntp // 2
    far = ny // 2
    s = lax.axis_index("sp")
    t = lax.axis_index("tp")
    z = lax.div(s, NX)
    y = lax.div(t, 2)
    c = lax.rem(t, 2)
    up_dev = (s, lax.rem(y + 1, ny) * 2 + c)
    down_dev = (s, lax.rem(y + ny - 1, ny) * 2 + c)
    pair_dev = (s, y * 2 + 1 - c)

    barrier = pltpu.get_barrier_semaphore()

    def greet_sp(i, _):
        pl.semaphore_signal(
            barrier, inc=1, device_id=(lax.rem(s + i, nsp), t), device_id_type=MESH
        )
        return 0

    def greet_tp(i, _):
        pl.semaphore_signal(
            barrier, inc=1, device_id=(s, lax.rem(t + i, ntp)), device_id_type=MESH
        )
        return 0

    lax.fori_loop(1, nsp, greet_sp, 0)
    lax.fori_loop(1, ntp, greet_tp, 0)

    w_copies = [
        pltpu.make_async_copy(wg_hbm.at[0], wg, w_sem.at[0]),
        pltpu.make_async_copy(wu_hbm.at[0], wu, w_sem.at[1]),
        pltpu.make_async_copy(wd_hbm.at[0], wd, w_sem.at[2]),
    ]
    for copy in w_copies:
        copy.start()

    tok = moe_ref.shape[0]
    slots = nsp * SLOTS
    eye = lax.broadcasted_iota(jnp.int32, (tok, tok), 0) == lax.broadcasted_iota(
        jnp.int32, (tok, tok), 1
    )
    before = lax.broadcasted_iota(jnp.int32, (tok, tok), 1) < lax.broadcasted_iota(
        jnp.int32, (tok, tok), 0
    )
    expert_lane = lax.broadcasted_iota(jnp.int32, (tok, 128), 1)
    hot = [(routes_ref[:, k : k + 1] == expert_lane).astype(F32) for k in range(2)]
    counts = nn(
        jnp.where(before, 1.0, 0.0).astype(BF16), (hot[0] + hot[1]).astype(BF16)
    )
    target_col = [
        jnp.sum(hot[k] * counts, axis=1, keepdims=True)
        + SLOTS * routes_ref[:, k : k + 1].astype(F32)
        for k in range(2)
    ]
    slot_row = lax.broadcasted_iota(jnp.int32, (slots, tok), 0).astype(F32)
    place = [
        jnp.where(
            slot_row == jnp.sum(jnp.where(eye, target_col[k], 0.0), axis=0, keepdims=True), 1.0, 0.0
        ).astype(BF16)
        for k in range(2)
    ]
    cot = cot_ref[...]
    cot_f = cot.astype(F32)
    rows = nn(place[0] + place[1], moe_ref[...])
    weighted = nn(place[0], (rw_ref[:, 0:1] * cot_f).astype(BF16)) + nn(
        place[1], (rw_ref[:, 1:2] * cot_f).astype(BF16)
    )
    pack[:, 0:SLOTS, :] = rows.astype(BF16).reshape(nsp, SLOTS, 128)
    pack[:, SLOTS : 2 * SLOTS, :] = weighted.astype(BF16).reshape(nsp, SLOTS, 128)

    pl.semaphore_wait(barrier, nsp + ntp - 2)

    def dz(k):
        odd = lax.rem(k, 2)
        return odd * lax.div(k + 1, 2) + (1 - odd) * lax.rem(nz - lax.div(k, 2), nz)

    def peer(k, i):
        return lax.rem(z + dz(k), nz) * NX + lax.rem(s + i, NX)

    def send_rows(k, _):
        for i in range(NX):
            e = peer(k, i)

            @pl.when(e != s)
            def _():
                rcopy(pack.at[e], gath.at[t, s], a2a_s.at[e], a2a_r.at[s], (e, t)).start()

        return 0

    lax.fori_loop(0, nz, send_rows, 0)
    gath[t, s] = pack[s]

    def part_of(r):
        return lax.rem(y + ny - r, ny) * 2 + c

    def piece(r, k):
        zs = lax.rem(z + nz - dz(k), nz)
        return gath.at[part_of(r), pl.ds(zs * NX, NX)]

    def to_up(r, k):
        return rcopy(piece(r, k), piece(r, k), cw_s.at[r, k], nb_r.at[r + 1, k], up_dev)

    def to_down(r, k):
        return rcopy(
            piece(r, k), piece(r, k), ccw_s.at[r, k], nb_r.at[(r + ny - 1) % ny, k], down_dev
        )

    def to_pair(r, k):
        return rcopy(piece(r, k), piece(r, k), par_s.at[r, k], par_r.at[r, k], pair_dev)

    def from_nb(r, k):
        rcopy(piece(r, k), piece(r, k), cw_s.at[r, k], nb_r.at[r, k], up_dev).wait_recv()

    def own_stage(k, _):
        zs = lax.rem(z + nz - dz(k), nz)
        for i in range(NX):
            e = zs * NX + i

            @pl.when(e != s)
            def _():
                rcopy(pack.at[e], gath.at[t, e], a2a_s.at[e], a2a_r.at[e], (e, t)).wait_recv()

        to_up(0, k).start()
        to_down(0, k).start()
        to_pair(0, k).start()
        return 0

    lax.fori_loop(0, nz, own_stage, 0)

    def send_wp(k, _):
        for i in range(NX):
            e = peer(k, i)

            @pl.when(e != s)
            def _():
                rcopy(wproj_ref, wp.at[s], wp_s.at[e], wp_r.at[s], (e, t)).start()

        return 0

    lax.fori_loop(0, nz, send_wp, 0)
    wp[s] = wproj_ref[...]

    acc_g[...] = jnp.zeros_like(acc_g)
    acc_u[...] = jnp.zeros_like(acc_u)
    acc_h[...] = jnp.zeros_like(acc_h)
    for copy in w_copies:
        copy.wait()

    def stage(h):
        def body(kk, _):
            for odd in range(2):
                k = 2 * kk + odd
                for cw in (True, False):
                    reach = far if cw != bool(odd) else ny - 1 - far
                    if h > reach:
                        continue
                    r = h if cw else ny - h
                    from_nb(r, k)
                    if h < reach:
                        (to_up(r, k) if cw else to_down(r, k)).start()
                    to_pair(r, k).start()
            return 0

        lax.fori_loop(0, nz // 2, body, 0)

    def chip_rows(yp, lo):
        return jnp.concatenate(
            [
                gath[2 * yp, :, lo : lo + SLOTS, :].reshape(slots, 128),
                gath[2 * yp + 1, :, lo : lo + SLOTS, :].reshape(slots, 128),
            ],
            axis=1,
        )

    def contract(rs):
        def one(r):
            def arrived(k, _):
                rcopy(
                    piece(r, k),
                    gath.at[
                        lax.rem(y + ny - r, ny) * 2 + 1 - c,
                        pl.ds(lax.rem(z + nz - dz(k), nz) * NX, NX),
                    ],
                    par_s.at[r, k],
                    par_r.at[r, k],
                    pair_dev,
                ).wait_recv()
                return 0

            lax.fori_loop(0, nz, arrived, 0)
            yp = lax.rem(y + ny - r, ny)
            cols = pl.ds(pl.multiple_of(yp * 256, 256), 256)
            a = chip_rows(yp, 0)
            acc_g[...] += nt(a, wg[:, cols])
            acc_u[...] += nt(a, wu[:, cols])
            acc_h[...] += nt(chip_rows(yp, SLOTS), wd[:, cols])

        for r in rs:
            one(r)

    for h in range(1, far + 1):
        stage(h)
        contract([0] if h == 1 else [h - 1, ny - h + 1])
    contract([far])

    gate_pre = acc_g[...]
    up_pre = acc_u[...]
    hidden_grad = acc_h[...]
    gate_sig = sigmoid(gate_pre)
    gate_active = gate_pre * gate_sig
    gg[...] = (hidden_grad * up_pre * silu_slope(gate_pre, gate_sig)).astype(BF16)
    ug[...] = (hidden_grad * gate_active).astype(BF16)
    hid[...] = (gate_active * up_pre).astype(BF16)

    def to_partner(d):
        return rcopy(d2d_out.at[d], d2d_in.at[d], d2_s.at[d], d2_r.at[d], pair_dev)

    def partials(ds):
        for d in ds:
            yp = lax.rem(y + d, ny)
            cols = pl.ds(pl.multiple_of(yp * 256, 256), 256)
            both = nn(gg[...], wg[:, cols]) + nn(ug[...], wu[:, cols])
            first, second = both[:, :128], both[:, 128:]
            mine[d] = jnp.where(c == 0, first, second)
            d2d_out[d] = jnp.where(c == 0, second, first).astype(BF16)
            to_partner(d).start()

    row_count = NX * SLOTS

    def block(k):
        zd = lax.rem(z + dz(k), nz)
        return pl.ds(pl.multiple_of(zd * row_count, row_count), row_count)

    def ring(d):
        def body(kk, _):
            for odd in range(2):
                k = 2 * kk + odd
                at = block(k)
                for cw in (True, False):
                    reach = far if cw != bool(odd) else ny - 1 - far
                    if d > reach:
                        continue
                    rel = d if cw else ny - d
                    got, out = (cw_in, cw_out) if cw else (ccw_in, ccw_out)
                    ssem, rsem = (rcw_s, rcw_r) if cw else (rccw_s, rccw_r)
                    dev = up_dev if cw else down_dev
                    val = mine[rel, at, :] + d2d_in[rel, at, :].astype(F32)
                    if d < reach:
                        rcopy(
                            out.at[d, at], got.at[d, at], ssem.at[d, k], rsem.at[d, k], dev
                        ).wait_recv()
                        val = val + got[d, at, :].astype(F32)
                    out[d, at, :] = val.astype(BF16)
                    rcopy(
                        out.at[d, at], got.at[d - 1, at], ssem.at[d, k], rsem.at[d - 1, k], dev
                    ).start()
            return 0

        lax.fori_loop(0, nz // 2, body, 0)

    def pair_ready(ds):
        for d in ds:
            to_partner(d).wait_recv()

    partials([far])
    partials([far - 1, ny - far + 1])
    pair_ready([far])
    ring(far)
    for d in range(far - 1, 0, -1):
        partials([d - 1] if d == 1 else [d - 1, ny - d + 1])
        pair_ready([d, ny - d])
        ring(d)
    pair_ready([0])

    def finish(k, _):
        at = block(k)
        rcopy(cw_out.at[1, at], cw_in.at[0, at], rcw_s.at[1, k], rcw_r.at[0, k], up_dev).wait_recv()
        rcopy(
            ccw_out.at[1, at], ccw_in.at[0, at], rccw_s.at[1, k], rccw_r.at[0, k], down_dev
        ).wait_recv()
        val = (
            mine[0, at, :]
            + d2d_in[0, at, :].astype(F32)
            + cw_in[0, at, :].astype(F32)
            + ccw_in[0, at, :].astype(F32)
        )
        zd = lax.rem(z + dz(k), nz)
        fin[pl.ds(zd * NX, NX)] = val.astype(BF16).reshape(NX, SLOTS, 128)
        for i in range(NX):
            e = peer(k, i)

            @pl.when(e != s)
            def _():
                rcopy(fin.at[e], back.at[s], ret_s.at[e], ret_r.at[s], (e, t)).start()

        return 0

    lax.fori_loop(0, nz, finish, 0)
    back[s] = fin[s]

    hid_t = hid[...].T
    ug_t = ug[...].T

    def weight_grads(yp, _):
        cols = pl.ds(pl.multiple_of(yp * 256, 256), 256)
        gdown[:, cols] = nn(hid_t, chip_rows(yp, SLOTS)).astype(BF16)
        gup[:, cols] = nn(ug_t, chip_rows(yp, 0)).astype(BF16)
        return 0

    lax.fori_loop(0, ny, weight_grads, 0)
    out_copies = [
        pltpu.make_async_copy(gup, gup_hbm.at[0], out_sem.at[0]),
        pltpu.make_async_copy(gdown, gdown_hbm.at[0], out_sem.at[1]),
    ]
    for copy in out_copies:
        copy.start()

    normed = (conv_ref[...].astype(F32) - mean_ref[...]) * rstd_ref[...]
    pre_act = normed * gain_ref[...] + shift_ref[...]
    act_sig = sigmoid(pre_act)
    activated = (pre_act * act_sig).astype(BF16)
    slope = silu_slope(pre_act, act_sig) * gain_ref[...]

    def returned(e, _):
        @pl.when(e != s)
        def _():
            rcopy(fin.at[e], back.at[e], ret_s.at[e], ret_r.at[e], (e, t)).wait_recv()

        return 0

    lax.fori_loop(0, nsp, returned, 0)
    slot_lane = lax.broadcasted_iota(jnp.int32, (tok, slots), 1).astype(F32)
    pick = jnp.where((slot_lane == target_col[0]) | (slot_lane == target_col[1]), 1.0, 0.0)
    grad_stream = (cot_f + nn(pick.astype(BF16), back[...].reshape(slots, 128))).astype(BF16)
    gs_out[...] = grad_stream
    gsa[t] = grad_stream

    step = tok // GP

    def gpiece(r, k, other=False):
        part = lax.rem(y + ny - r, ny) * 2 + (1 - c if other else c)
        return gsa.at[part, pl.ds(k * step, step)]

    def g_up(r, k):
        return rcopy(gpiece(r, k), gpiece(r, k), gcw_s.at[r, k], gn_r.at[r + 1, k], up_dev)

    def g_down(r, k):
        return rcopy(
            gpiece(r, k), gpiece(r, k), gccw_s.at[r, k], gn_r.at[(r + ny - 1) % ny, k], down_dev
        )

    def g_pair(r, k):
        return rcopy(gpiece(r, k), gpiece(r, k), gpar_s.at[r, k], gpar_r.at[r, k], pair_dev)

    def g_from(r, k):
        rcopy(gpiece(r, k), gpiece(r, k), gcw_s.at[r, k], gn_r.at[r, k], up_dev).wait_recv()

    for k in range(GP):
        g_up(0, k).start()
        g_down(0, k).start()
        g_pair(0, k).start()

    def wp_arrived(e, _):
        @pl.when(e != s)
        def _():
            rcopy(wproj_ref, wp.at[e], wp_s.at[e], wp_r.at[e], (e, t)).wait_recv()

        return 0

    lax.fori_loop(0, nsp, wp_arrived, 0)
    w_rows = wp.shape[1]
    chunk = 256 // w_rows

    def g_stage(h):
        for k in range(GP):
            for cw in (True, False):
                reach = far if cw != bool(k % 2) else ny - 1 - far
                if h > reach:
                    continue
                r = h if cw else ny - h
                g_from(r, k)
                if h < reach:
                    (g_up(r, k) if cw else g_down(r, k)).start()
                g_pair(r, k).start()

    def g_contract(rs, total):
        for r in rs:
            for k in range(GP):
                rcopy(
                    gpiece(r, k), gpiece(r, k, True), gpar_s.at[r, k], gpar_r.at[r, k], pair_dev
                ).wait_recv()
            yp = lax.rem(y + ny - r, ny)
            a = jnp.concatenate([gsa[2 * yp], gsa[2 * yp + 1]], axis=1)
            total = total + nn(a, wp[pl.ds(yp * chunk, chunk)].reshape(256, 128))
            gp[pl.ds(yp * chunk, chunk)] = tn(a, activated).astype(BF16).reshape(
                chunk, w_rows, 128
            )
        return total

    act_grad = jnp.zeros((tok, 128), F32)
    for h in range(1, far + 1):
        g_stage(h)
        act_grad = g_contract([0] if h == 1 else [h - 1, ny - h + 1], act_grad)
    act_grad = g_contract([far], act_grad)

    ng = act_grad * slope
    ng_n = ng * normed
    ones = jnp.ones((8, 128), F32)

    def row_sums(v):
        return lax.dot_general(
            ones,
            v,
            (((1,), (1,)), ((), ())),
            preferred_element_type=F32,
            precision=lax.Precision.HIGHEST,
        )[0:1]

    sums[t] = jnp.concatenate([row_sums(ng), row_sums(ng_n)], axis=0)

    def send_sums(i, _):
        o = lax.rem(t + i, ntp)
        rcopy(sums.at[t], sums.at[t], ar_s.at[o], ar_r.at[t], (s, o)).start()
        return 0

    lax.fori_loop(1, ntp, send_sums, 0)

    def send_gp(k, _):
        for i in range(NX):
            e = peer(k, i)

            @pl.when(e != s)
            def _():
                rcopy(gp.at[e], gr.at[s], gp_s.at[e], gp_r.at[s], (e, t)).start()

        return 0

    lax.fori_loop(0, nz, send_gp, 0)
    gr[s] = gp[s]

    def sums_arrived(i, _):
        o = lax.rem(t + i, ntp)
        rcopy(sums.at[o], sums.at[o], ar_s.at[o], ar_r.at[o], (s, o)).wait_recv()
        return 0

    lax.fori_loop(1, ntp, sums_arrived, 0)
    total = jnp.sum(sums[...], axis=0) * (1.0 / (ntp * 128))
    mean_col = [
        jnp.sum(jnp.where(eye, total[k : k + 1, :], 0.0), axis=1, keepdims=True) for k in range(2)
    ]
    conv_grad = rstd_ref[...] * (ng - mean_col[0] - normed * mean_col[1])
    ext[0:tok, :] = conv_grad

    prev_dev = (lax.rem(s + nsp - 1, nsp), t)
    rim = rcopy(ext.at[pl.ds(0, 32)], rim_in, rim_s, rim_r, prev_dev)
    rim.start()
    rim.wait_recv()
    ext[tok : tok + 32, :] = jnp.where(s == nsp - 1, 0.0, rim_in[...])
    conv = jnp.zeros((tok, 128), F32)
    for lag in range(taps_ref.shape[0]):
        conv = conv + taps_ref[lag : lag + 1, :] * ext[lag : lag + tok, :]
    gconv_out[...] = conv.astype(BF16)

    def gp_arrived(e, _):
        @pl.when(e != s)
        def _():
            rcopy(gp.at[e], gr.at[e], gp_s.at[e], gp_r.at[e], (e, t)).wait_recv()

        return 0

    lax.fori_loop(0, nsp, gp_arrived, 0)

    def add_gp(e, v):
        return v + gr[e].astype(F32)

    gproj_out[...] = lax.fori_loop(0, nsp, add_gp, jnp.zeros((w_rows, 128), F32))

    rim.wait_send()
    for copy in out_copies:
        copy.wait()

    def drain_sp(e, _):
        @pl.when(e != s)
        def _():
            rcopy(pack.at[e], gath.at[t, s], a2a_s.at[e], a2a_r.at[s], (e, t)).wait_send()
            rcopy(wproj_ref, wp.at[s], wp_s.at[e], wp_r.at[s], (e, t)).wait_send()
            rcopy(fin.at[e], back.at[s], ret_s.at[e], ret_r.at[s], (e, t)).wait_send()
            rcopy(gp.at[e], gr.at[s], gp_s.at[e], gp_r.at[s], (e, t)).wait_send()

        return 0

    lax.fori_loop(0, nsp, drain_sp, 0)

    def drain_tp(i, _):
        o = lax.rem(t + i, ntp)
        rcopy(sums.at[t], sums.at[t], ar_s.at[o], ar_r.at[t], (s, o)).wait_send()
        return 0

    lax.fori_loop(1, ntp, drain_tp, 0)
    for d in range(ny):
        to_partner(d).wait_send()

    def drain_pieces(kk, _):
        for odd in range(2):
            k = 2 * kk + odd
            at = block(k)
            for r in range(ny):
                to_pair(r, k).wait_send()
            for cw in (True, False):
                reach = far if cw != bool(odd) else ny - 1 - far
                for h in range(reach):
                    r = h if cw else (ny - h) % ny
                    (to_up(r, k) if cw else to_down(r, k)).wait_send()
                for d in range(1, reach + 1):
                    if cw:
                        rcopy(
                            cw_out.at[d, at], cw_in.at[d - 1, at], rcw_s.at[d, k], rcw_r.at[d - 1, k], up_dev
                        ).wait_send()
                    else:
                        rcopy(
                            ccw_out.at[d, at], ccw_in.at[d - 1, at], rccw_s.at[d, k], rccw_r.at[d - 1, k], down_dev
                        ).wait_send()
        return 0

    lax.fori_loop(0, nz // 2, drain_pieces, 0)
    for k in range(GP):
        for r in range(ny):
            g_pair(r, k).wait_send()
        for cw in (True, False):
            reach = far if cw != bool(k % 2) else ny - 1 - far
            for h in range(reach):
                r = h if cw else (ny - h) % ny
                (g_up(r, k) if cw else g_down(r, k)).wait_send()


def on_device(
    moe_in,
    cotangent,
    routes,
    route_weight,
    w_gate,
    w_up,
    w_down,
    conv_pre,
    norm_mean,
    norm_rstd,
    ln_gain,
    ln_shift,
    taps,
    w_proj,
):
    nsp = lax.axis_size("sp")
    ntp = lax.axis_size("tp")
    nz = nsp // NX
    ny = ntp // 2
    far = ny // 2
    tok = moe_in.shape[0]
    ff, width = w_gate.shape[1:]
    slots = nsp * SLOTS
    w_rows = w_proj.shape[0]
    vmem = pl.BlockSpec(memory_space=pltpu.VMEM)
    hbm = pl.BlockSpec(memory_space=pl.ANY)
    dma = pltpu.SemaphoreType.DMA
    return pl.pallas_call(
        functools.partial(kernel, nsp, ntp),
        out_shape=(
            jax.ShapeDtypeStruct(w_up.shape, BF16),
            jax.ShapeDtypeStruct(w_down.shape, BF16),
            jax.ShapeDtypeStruct((tok, 128), BF16),
            jax.ShapeDtypeStruct((w_rows, 128), F32),
            jax.ShapeDtypeStruct((tok, 128), BF16),
        ),
        in_specs=[vmem] * 4 + [hbm] * 3 + [vmem] * 7,
        out_specs=(hbm, hbm, vmem, vmem, vmem),
        scratch_shapes=[
            pltpu.VMEM((nsp, 2 * SLOTS, 128), BF16),
            pltpu.VMEM((ntp, nsp, 2 * SLOTS, 128), BF16),
            pltpu.VMEM((ff, width), BF16),
            pltpu.VMEM((ff, width), BF16),
            pltpu.VMEM((ff, width), BF16),
            pltpu.VMEM((slots, ff), F32),
            pltpu.VMEM((slots, ff), F32),
            pltpu.VMEM((slots, ff), F32),
            pltpu.VMEM((slots, ff), BF16),
            pltpu.VMEM((slots, ff), BF16),
            pltpu.VMEM((slots, ff), BF16),
            pltpu.VMEM((ff, width), BF16),
            pltpu.VMEM((ff, width), BF16),
            pltpu.VMEM((ny, slots, 128), F32),
            pltpu.VMEM((ny, slots, 128), BF16),
            pltpu.VMEM((ny, slots, 128), BF16),
            pltpu.VMEM((far, slots, 128), BF16),
            pltpu.VMEM((far, slots, 128), BF16),
            pltpu.VMEM((far + 1, slots, 128), BF16),
            pltpu.VMEM((far + 1, slots, 128), BF16),
            pltpu.VMEM((nsp, SLOTS, 128), BF16),
            pltpu.VMEM((nsp, SLOTS, 128), BF16),
            pltpu.VMEM((nsp, w_rows, 128), BF16),
            pltpu.VMEM((ntp, tok, 128), BF16),
            pltpu.VMEM((nsp, w_rows, 128), BF16),
            pltpu.VMEM((nsp, w_rows, 128), BF16),
            pltpu.VMEM((ntp, 2, tok), F32),
            pltpu.VMEM((tok, 128), F32),
            pltpu.VMEM((tok + 32, 128), F32),
            pltpu.VMEM((32, 128), F32),
            dma((3,)),
            dma((2,)),
            dma((nsp,)),
            dma((nsp,)),
            dma((ny, nz)),
            dma((ny, nz)),
            dma((ny, nz)),
            dma((ny, nz)),
            dma((ny, nz)),
            dma((nsp,)),
            dma((nsp,)),
            dma((ny,)),
            dma((ny,)),
            dma((far + 1, nz)),
            dma((far + 1, nz)),
            dma((far, nz)),
            dma((far, nz)),
            dma((nsp,)),
            dma((nsp,)),
            dma((ny, GP)),
            dma((ny, GP)),
            dma((ny, GP)),
            dma((ny, GP)),
            dma((ny, GP)),
            dma((nsp,)),
            dma((nsp,)),
            dma((ntp,)),
            dma((ntp,)),
            dma,
            dma,
        ],
        compiler_params=pltpu.CompilerParams(
            collective_id=0, has_side_effects=True, vmem_limit_bytes=60 * 1024 * 1024
        ),
        name="layer_backward",
    )(
        moe_in,
        cotangent,
        routes,
        route_weight,
        w_gate,
        w_up,
        w_down,
        conv_pre,
        norm_mean[:, None],
        norm_rstd[:, None],
        ln_gain[None, :],
        ln_shift[None, :],
        taps,
        w_proj,
    )


def solution(mesh):
    placed = (
        P("sp", "tp"),
        P("sp", "tp"),
        P("sp", None),
        P("sp", None),
        P("sp", "tp", None),
        P("sp", "tp", None),
        P("sp", "tp", None),
        P("sp", "tp"),
        P("sp"),
        P("sp"),
        P("tp"),
        P("tp"),
        P(None, "tp"),
        P("sp", "tp"),
    )
    return jax.shard_map(
        on_device,
        mesh=mesh,
        in_specs=placed,
        out_specs=(
            P("sp", "tp", None),
            P("sp", "tp", None),
            P("sp", "tp"),
            P("sp", "tp"),
            P("sp", "tp"),
        ),
        check_vma=False,
    )
```

time: 248 us -> 120 us (0.48)
  waiting for transfers between devices: 116 us -> 0 us
  Pallas kernels: 0 us -> 110 us
  blocking collectives: 43.5 us -> 0 us
  starting transfers between devices: 35 us -> 0 us
  matrix products: 15.5 us -> 0 us
  between operations: 14.9 us -> 0.67 us
  local copies, waits for them, and re-layouts: 17 us -> 9.18 us
  other arithmetic: 5.23 us -> 0 us
    pallas_call x0 -> x1, Pallas kernels: none -> 110 us  [on_device(): pl.pallas_call(functools.partial(kernel, nsp, ntp), out_shape=(jax.ShapeD...]
    all_to_all x5 -> x0, waiting for transfers between devices: 65.9 us -> none  [the longest x2 52.3 us: summed_on_arrival(): lax.all_to_all(blocks, axis, split_axis=0, concat_axis=0, tiled=True)]
    all_gather x1 -> x0, waiting for transfers between devices: 49.1 us -> none  [side_by_side(): out = lax.all_gather(both, axis, axis=dim, tiled=True)]
    all_to_all x5 -> x0, starting transfers between devices: 33.7 us -> none  [the longest x2 13.2 us: summed_on_arrival(): lax.all_to_all(blocks, axis, split_axis=0, concat_axis=0, tiled=True)]
    all_to_all x1 -> x0, blocking collectives: 24.8 us -> none  [sent_together(): lax.all_to_all(both, axis, split_axis=split_dim, concat_axis=concat_dim,...]
    all_gather x1 -> x0, blocking collectives: 18.7 us -> none  [on_device(): mix_grad = lax.all_gather(grad_stream, 'tp', axis=1, tiled=True)]
    dot_general x9 -> x0, matrix products: 15.5 us -> none  [the longest x1 3.15 us: expert_backward(): lax.dot_general(hidden, routed_rows, (((0,), (0,)), ((), ())), preferred_...]
    gather x5 -> x0, local copies, waits for them, and re-layouts: 5.09 us -> none  [the longest x2 2.08 us: on_device(): jnp.take(moe_in, route_of_slot // top_count, axis=0)]
  transfers between devices with their start and end apart: 7 -> 0, of which waited for: 6 -> 0; matrix products, arithmetic and copies ran while one was open for 6% -> 0% of each run, Pallas kernels for 0% -> 0%
where the time goes in v1:
time: 120 us
  Pallas kernels  110 us (92%)
  local copies, waits for them, and re-layouts  9.18 us (8%)
    pallas_call x1, Pallas kernels, on_device(): pl.pallas_call(functools.partial(kernel, nsp, ntp), out_shape=(jax.ShapeD...  110 us
    unnamed x23, local copies, waits for them, and re-layouts  7.62 us

profile of v1, /device:TPU:1, one launch (start us, length us, event | category | flops | bytes accessed | tf_op | source)
XLA Modules:
  0.0 120.1 jit_solution(11292350893870686032)
XLA Ops:
  0.6 0.0 copy-start.4
  0.6 0.7 copy-done.4
  1.3 0.0 copy-start.5
  1.3 0.8 copy.21.routes_ref
  2.1 0.0 copy-done.5
  2.1 0.0 copy-start.6
  2.1 0.8 copy.22.rw_ref
  2.9 0.0 copy-done.6
  2.9 0.0 copy-start.7
  2.9 0.8 copy.23.mean_ref
  3.6 0.0 copy-done.7
  3.6 0.8 copy.24.rstd_ref
  4.4 110.3 %layer_backward.1 = (bf16[1,224,2048]{2,1,0:T(8,128)(2,1)}, bf16[1,224,2048]{2,1,0:T(8,128)(2,1)}, bf16[192,128]{1,0:T(8,128)(2,1)}, f32[64,128]{1,0:T(8,128)}, bf16[192,128]{1,0:T(8,128)(2,1)}) custom-call(bf16[192,128]{1,0:T(8,128)(2,1)} %moe_ref.1, bf16[192,128]{1,0:T(8,128)(2,1)} %cot_ref.1, s32[192,2]{1,0:T(8,128)} %copy.21.routes_ref, ...), custom_call_target="tpu_custom_call" | custom-call | tf_op jit(solution)/shard_map/layer_backward/pallas_call | solution.py:691
  114.7 0.0 copy-start
  114.7 2.3 %copy.30 = bf16[1,224,2048]{2,1,0:T(8,128)(2,1)} copy(bf16[1,224,2048]{2,1,0:T(8,128)(2,1)} %get-tuple-element.10) | data formatting | bytes 1835008
  117.0 0.0 copy-done
  117.0 0.0 copy-start.2
  117.0 0.9 copy.31
  117.9 0.0 copy-done.2
  118.0 0.6 copy.32
  118.6 0.1 copy-done.3
  118.7 0.6 copy.33
  119.3 0.2 copy-done.1
  119.5 0.6 copy.34
  (2 shorter events, 0.0 us)
Async XLA Ops:
  0.6 0.7 copy-start.4
  1.3 0.8 copy-start.5
  2.1 0.8 copy-start.6
  2.9 0.8 copy-start.7
  114.7 2.3 %copy-start = (bf16[1,224,2048]{2,1,0:T(8,128)(2,1)S(1)}, bf16[1,224,2048]{2,1,0:T(8,128)(2,1)}, u32[]{:S(2)}) copy-start(bf16[1,224,2048]{2,1,0:T(8,128)(2,1)} %get-tuple-element.11) | copy-start | bytes 2752516
  117.0 0.9 copy-start.2
  117.9 0.8 copy-start.3
  118.7 0.8 copy-start.1
